TPU v7x, 32 devices: a whole 2x2x4 slice. The times are simulated.
32 devices in a mesh: ep: 8 (over z, y), tp: 4 (over x, core).
Axes of the slice: x: 2, y: 2, z: 4, core: 2. Of those that a mesh axis runs over, the one named last changes fastest.
Arguments:
- mixer_in: bfloat16 [8192, 4096], P('ep', 'tp'), may hold values from -110 to 110
- mixer_gain: float32 [4096], P('tp'), may hold values from 0.1 to 1.9
- pool_weight: bfloat16 [4, 1024, 1024], P('tp'), may hold values from -0.1875 to 0.1875
- pool_scale: float32 [4096], P('tp'), may hold values from 0.1 to 1.9
- moe_in: bfloat16 [2048, 4096], P('ep'), may hold values from -6 to 6
- moe_gain: float32 [4096], replicated, may hold values from 0.1 to 1.9
- route_expert: int32 [2048, 2], P('ep'), may hold values from 0 to 7, as said below
- route_weight: float32 [2048, 2], P('ep'), may hold values from 0.1 to 1
- gate_weight: bfloat16 [8, 4096, 1024], P('ep', None, 'tp'), may hold values from -0.09375 to 0.09375
- up_weight: bfloat16 [8, 4096, 1024], P('ep', None, 'tp'), may hold values from -0.09375 to 0.09375
- down_weight: bfloat16 [8, 1024, 4096], P('ep', 'tp'), may hold values from -0.1875 to 0.1875
Outputs:
- mixer_out: bfloat16 [8192, 4096], P('ep', 'tp')
- moe_out: bfloat16 [2048, 4096], P('ep', 'tp')
Inputs may be any that keep to these rules, and one draw needn't show every extreme that they name: `route_expert`: both experts of a row are different and lie in one group: the group of an expert is its number divided by 2, rounded down. Among the rows of one index of ep no expert is named more than 96 times; in every draw the experts of some group are each named exactly 96 times by the rows of every index of ep.
All inputs are finite; a program needn't handle non-finite values.
Results may differ from a plain program's by a relative error of at most 0.0071.
Values may be sent and summed in bfloat16 or wider, within the bound.
A program may use at most 128 MiB of HBM per device.

v0:
```python
import jax
import jax.numpy as jnp
from jax import lax
from jax.sharding import PartitionSpec as P

D = 4096
WINDOW_MAX = 16


EPS = 1e-06


def passed_along(value, axis, steps):
    count = lax.axis_size(axis)
    first, last = (max(0, -steps), min(count, count - steps))
    return lax.ppermute(value, axis, [(source, source + steps) for source in range(first, last)])


def shards(
    mixer_in,
    mixer_gain,
    pool_weight,
    pool_scale,
    moe_in,
    moe_gain,
    route_expert,
    route_weight,
    gate_weight,
    up_weight,
    down_weight,
):
    rows = mixer_in.shape[0]
    feats = mixer_in.astype(jnp.float32)
    squares = lax.psum(jnp.sum(feats * feats, axis=1), "tp")
    normed_a = (feats * lax.rsqrt(squares[:, None] / D + EPS) * mixer_gain).astype(jnp.bfloat16)
    reach = WINDOW_MAX - 1
    before = passed_along(normed_a[rows - reach :], "ep", 1)
    extended = jnp.concatenate([before, normed_a], axis=0).astype(jnp.float32)
    running = jnp.zeros((rows, normed_a.shape[1]), jnp.float32)
    totals = []
    for offset in range(WINDOW_MAX):
        running = running + lax.slice_in_dim(
            extended, reach - offset, reach - offset + rows, axis=0
        )
        if offset > 0 and offset + 1 & offset == 0:
            totals.append(running)
    group = lax.axis_index("tp")
    window_sum = lax.dynamic_index_in_dim(jnp.stack(totals), group, 0, keepdims=False)
    span = jnp.left_shift(jnp.int32(2), group)
    position = lax.axis_index("ep") * rows + jnp.arange(rows, dtype=jnp.int32)
    count = jnp.minimum(position + 1, span).astype(jnp.float32)[:, None]
    pooled = (window_sum / count - extended[reach:]).astype(jnp.bfloat16)
    mixer_out = (
        jnp.dot(pooled, pool_weight[0], preferred_element_type=jnp.float32) * pool_scale
    ).astype(jnp.bfloat16)
    tokens = moe_in.shape[0]
    feats_b = moe_in.astype(jnp.float32)
    normed_b = (
        feats_b * lax.rsqrt(jnp.mean(feats_b * feats_b, axis=1, keepdims=True) + EPS) * moe_gain
    ).astype(jnp.bfloat16)
    experts = gate_weight.shape[0] * lax.axis_size("ep")
    slots = 3 * tokens // experts
    flat = route_expert.reshape(-1)
    onehot = (flat[:, None] == jnp.arange(experts, dtype=jnp.int32)[None, :]).astype(jnp.int32)
    earlier = jnp.cumsum(onehot, axis=0) - onehot
    slot_index = flat * slots + jnp.sum(earlier * onehot, axis=1)
    owner = jnp.arange(2 * tokens, dtype=jnp.int32) // 2
    source = jnp.full((experts * slots,), tokens, jnp.int32).at[slot_index].set(owner)
    padded_b = jnp.concatenate([normed_b, jnp.zeros((1, D), jnp.bfloat16)], axis=0)
    outgoing = jnp.take(padded_b, source, axis=0).reshape(experts, slots, D)
    w_gate = gate_weight[0]
    w_up = up_weight[0]
    share = slots // lax.axis_size("tp")
    mine = lax.dynamic_slice_in_dim(outgoing, lax.axis_index("tp") * share, share, 1)
    arrived = lax.all_to_all(mine, "ep", split_axis=0, concat_axis=0, tiled=True)
    expand_arrived = lax.all_gather(arrived, "tp", axis=1, tiled=True)
    gate = jnp.einsum("nkd,df->nkf", expand_arrived, w_gate, preferred_element_type=jnp.float32)
    upper = jnp.einsum("nkd,df->nkf", expand_arrived, w_up, preferred_element_type=jnp.float32)
    hidden = (jax.nn.silu(gate) * upper).astype(jnp.bfloat16)
    flat_hidden = hidden.reshape(-1, hidden.shape[2])
    w_down = down_weight[0]
    columns = D // lax.axis_size("tp")
    summed = lax.psum_scatter(
        lax.dot_general(
            w_down, flat_hidden, (((0,), (1,)), ((), ())), preferred_element_type=jnp.float32
        ),
        "tp",
        scatter_dimension=0,
        tiled=True,
    ).astype(jnp.bfloat16)
    back = lax.all_to_all(
        summed.reshape(columns, -1, slots), "ep", split_axis=1, concat_axis=1, tiled=True
    )
    picked = jnp.take(back.reshape(columns, experts * slots), slot_index, axis=1)
    weighted = picked.astype(jnp.float32).reshape(columns, tokens, 2) * route_weight[None, :, :]
    moe_out = jnp.sum(weighted, axis=2).T.astype(jnp.bfloat16)
    return (mixer_out, moe_out)


def solution(mesh):
    return jax.shard_map(
        shards,
        mesh=mesh,
        in_specs=(
            P("ep", "tp"),
            P("tp"),
            P("tp", None, None),
            P("tp"),
            P("ep", None),
            P(),
            P("ep", None),
            P("ep", None),
            P("ep", None, "tp"),
            P("ep", None, "tp"),
            P("ep", "tp", None),
        ),
        out_specs=(P("ep", "tp"), P("ep", "tp")),
        check_vma=False,
    )
```

profile of v0, /device:TPU:0, one launch (start us, length us, event | category | flops | bytes accessed | tf_op | source)
XLA Modules:
  0.0 301.1 jit_solution(9724632331461842355)
XLA Ops:
  11.0 2.4 scatter_custom_fusion
  13.5 2.1 fusion.3
  15.7 2.2 fusion.5
  17.9 1.6 concatenate.7
  19.4 13.9 %gather_fusion = bf16[768,4096]{1,0:T(8,128)(2,1)} fusion(bf16[257,4096]{1,0:T(8,128)(2,1)} %concatenate.7, s32[1024]{0:T(1024)S(1)} %pad_clamp_fusion.1), kind=kCustom, calls=%fused_computation | custom fusion | bytes 12585984 | tf_op jit(solution)/shard_map/jit(_take)/gather | solution.py:70
  33.4 1.8 dynamic-slice_select_fusion
  35.2 44.2 %all_to_all.10 = bf16[8,24,4096]{2,1,0:T(8,128)(2,1)} all-to-all(bf16[8,24,4096]{2,1,0:T(8,128)(2,1)S(1)} %dynamic-slice_select_fusion), channel_id=1, replica_groups=mesh['ep'=8,'tp'=4] {'ep'}, dimensions={0} | all-to-all | bytes 3145728 | tf_op jit(solution)/shard_map/all_to_all | solution.py:75
  79.6 45.3 %all-gather.2.cloned.1.call-done = bf16[8,96,4096]{2,1,0:T(8,128)(2,1)} async-done(((bf16[8,24,4096]{2,1,0:T(8,128)(2,1)}), bf16[8,96,4096]{2,1,0:T(8,128)(2,1)}) %all-gather.2.cloned.1.call-update) | async-done | bytes 6291472 | tf_op jit(solution)/shard_map/all_gather | solution.py:76
  124.9 5.3 %fusion.17 = f32[8,96,256]{2,1,0:T(8,128)S(1)} fusion(bf16[8,96,4096]{2,1,0:T(8,128)(2,1)} %all-gather.2.cloned.1.call-done, bf16[1,4096,256]{2,1,0:T(8,128)(2,1)} %param.19), kind=kOutput, calls=%fused_computation.46 | convolution fusion | flops 1610612736 | bytes 9175040 | tf_op jit(solution)/shard_map/nkd,df->nkf/dot_general | solution.py:77
  130.8 1.8 fusion.25
  132.6 6.4 %convolution_bitcast_fusion = f32[4096,768]{0,1:T(8,128)} fusion(bf16[768,256]{1,0:T(8,128)(2,1)S(1)} %bitcast.65, bf16[1,256,4096]{2,1,0:T(8,128)(2,1)S(1)} %copy-done), kind=kOutput, calls=%fused_computation.7 | convolution fusion | flops 1610612736 | bytes 15073280 | tf_op jit(solution)/shard_map/dot_general | solution.py:84
  139.0 1.6 copy-done.2
  141.1 5.9 %psum.7 = f32[1024]{0:T(1024)S(1)} all-reduce(f32[1024]{0:T(1024)S(1)} %fusion), channel_id=1, replica_groups=mesh['ep'=8,'tp'=4] {'tp'}, use_global_device_ids=true, to_apply=%region_1.0 | all-reduce | flops 1024 | bytes 8192 | tf_op jit(solution)/shard_map/psum | solution.py:34
  147.0 2.9 fusion.2
  149.9 3.5 %collective-permute-start = (bf16[15,1024]{1,0:T(8,128)(2,1)S(1)}, bf16[15,1024]{1,0:T(8,128)(2,1)S(1)}, u32[]{:S(2)}, u32[]{:S(2)}) collective-permute-start(bf16[15,1024]{1,0:T(8,128)(2,1)S(1)} %slice.81), channel_id=1, source_target_pairs={{0,4},{4,8},{8,12},{12,16},{16,20},{20,24},{24,28},{1,5},{5,9},{9,... | collective-permute-start | bytes 92168 | tf_op jit(solution)/shard_map/ppermute | solution.py:16
  155.0 2.6 maximum_convert_fusion
  157.6 78.7 %reduce-scatter.2.cloned.1.call-done = f32[1024,768]{0,1:T(8,128)} async-done(((f32[4096,768]{0,1:T(8,128)}), f32[1024,768]{0,1:T(8,128)}) %reduce-scatter.2.cloned.1.call-update) | async-done | bytes 3145744 | tf_op jit(solution)/shard_map/reduce_scatter | solution.py:83
  236.3 3.3 %convert_element_type.62 = bf16[1024,768]{0,1:T(8,128)(2,1)} convert(f32[1024,768]{0,1:T(8,128)} %reduce-scatter.2.cloned.1.call-done) | non-fusion elementwise | flops 786432 | bytes 4718592 | tf_op jit(solution)/shard_map/convert_element_type | solution.py:90
  239.6 5.6 %all-to-all-start.1 = ((bf16[1024,8,96]{0,2,1:T(8,128)(2,1)}), bf16[1024,8,96]{0,2,1:T(8,128)(2,1)}, u32[]{:S(2)}, u32[]{:S(2)}) async-start(bf16[1024,8,96]{0,2,1:T(8,128)(2,1)} %bitcast.18), calls=%async_computation.2 | async-start | bytes 3145728 | tf_op jit(solution)/shard_map/all_to_all | solution.py:91
  245.3 28.7 %fusion.12 = (f32[1,1024,1024]{2,1,0:T(8,128)S(1)}, f32[1024,1024]{1,0:T(8,128)}, f32[1024,1024]{1,0:T(8,128)}, f32[1,1024,1024]{2,1,0:T(8,128)}) fusion(f32[1039,1024]{1,0:T(8,128)} %maximum_convert_fusion), kind=kLoop, calls=%fused_computation.25 | loop fusion | flops 15728640 | bytes 83886080 | tf_op jit(solution)/shard_map/stack | solution.py:48
  274.1 6.5 %multiply_convert_fusion = bf16[1024,1024]{1,0:T(8,128)(2,1)} fusion(bf16[1,1024,1024]{2,1,0:T(8,128)(2,1)S(1)} %copy-done.8, f32[1024]{0:T(1024)S(1)} %copy-done.9, s32[]{:T(128)S(6)} %select_n.44, f32[1,1024,1024]{2,1,0:T(8,128)S(1)} %get-tuple-element.2, f32[1,1024,1024]{2,1,0:T(8,128)} %bitcast.61, f32[1,1024,1024]{2,1,0:T(8,128)} %bitcast.62, ...), kind=kOutput, calls=%fused_computation.40 | convolution fusion | flops 2155872256 | bytes 25174020 | tf_op jit(solution)/shard_map/dot_general | solution.py:54
  280.6 1.6 all-to-all-done.1
  282.2 4.5 %gather_fusion.1 = bf16[512,1024]{1,0:T(8,128)(2,1)S(1)} fusion(bf16[1024,768]{0,1:T(8,128)(2,1)} %bitcast.19, s32[1024]{0:T(1024)S(1)} %pad_clamp_fusion), kind=kCustom, calls=%fused_computation.1 | custom fusion | bytes 2099200 | tf_op jit(solution)/shard_map/jit(_take)/gather | solution.py:94
  288.0 6.3 %multiply_reduce_fusion = bf16[1024,256]{0,1:T(8,128)(2,1)} fusion(bf16[1024,256,2]{0,2,1:T(2,128)(2,1)} %gather.15, pred[256,2]{1,0:T(8,128)(4,1)S(1)} %copy.22, f32[256,2]{1,0:T(8,128)S(1)} %copy.24), kind=kLoop, calls=%fused_computation.49 | loop fusion | flops 1835008 | bytes 1575424 | tf_op jit(solution)/shard_map/reduce_sum | solution.py:96
  (60 shorter events, 7.9 us)
Async XLA Ops:
  7.2 125.4 %copy-start = (bf16[1,256,4096]{2,1,0:T(8,128)(2,1)S(1)}, bf16[1,256,4096]{2,1,0:T(8,128)(2,1)}, u32[]{:S(2)}) copy-start(bf16[1,256,4096]{2,1,0:T(8,128)(2,1)} %param.21) | copy-start | bytes 6291460
  7.2 117.8 %all-gather.2.cloned.1.call-start = ((), (), s32[]{:S(2)}) async-start(), calls=%async_computation.3 | async-start | bytes 7864320 | tf_op jit(solution)/shard_map/all_gather | solution.py:76
  79.4 156.9 %reduce-scatter.2.cloned.1.call-start = ((), (), s32[]{:S(2)}) async-start(), calls=%async_computation.4 | async-start | bytes 15728640 | tf_op jit(solution)/shard_map/reduce_scatter | solution.py:83
  124.9 5.4 %copy-start.6 = (bf16[8,96,4096]{2,1,0:T(8,128)(2,1)S(1)}, bf16[8,96,4096]{2,1,0:T(8,128)(2,1)}, u32[]{:S(2)}) copy-start(bf16[8,96,4096]{2,1,0:T(8,128)(2,1)} %all-gather.2.cloned.1.call-done) | copy-start | bytes 18874372
  124.9 5.8 %copy-start.7 = (bf16[1,4096,256]{2,1,0:T(8,128)(2,1)S(1)}, bf16[1,4096,256]{2,1,0:T(8,128)(2,1)}, u32[]{:S(2)}) copy-start(bf16[1,4096,256]{2,1,0:T(8,128)(2,1)} %param.20) | copy-start | bytes 6291460
  139.0 1.6 copy-start.2
  139.0 8.0 %copy-start.4 = (f32[1024]{0:T(1024)S(1)}, f32[1024]{0:T(1024)}, u32[]{:S(2)}) copy-start(f32[1024]{0:T(1024)} %param.12) | copy-start | bytes 12292
  140.6 13.1 %copy-start.3 = (s32[256,2]{0,1:T(2,128)S(1)}, s32[256,2]{0,1:T(2,128)}, u32[]{:S(2)}) copy-start(s32[256,2]{0,1:T(2,128)} %param.17) | copy-start | bytes 6148
  140.6 13.3 %copy-start.5 = (f32[256,2]{0,1:T(2,128)S(1)}, f32[256,2]{0,1:T(2,128)}, u32[]{:S(2)}) copy-start(f32[256,2]{0,1:T(2,128)} %param.18) | copy-start | bytes 6148
  149.9 5.1 %collective-permute-start = (bf16[15,1024]{1,0:T(8,128)(2,1)S(1)}, bf16[15,1024]{1,0:T(8,128)(2,1)S(1)}, u32[]{:S(2)}, u32[]{:S(2)}) collective-permute-start(bf16[15,1024]{1,0:T(8,128)(2,1)S(1)} %slice.81), channel_id=1, source_target_pairs={{0,4},{4,8},{8,12},{12,16},{16,20},{20,24},{24,28},{1,5},{5,9},{9,... | collective-permute-start | bytes 92168 | tf_op jit(solution)/shard_map/ppermute | solution.py:16
  239.6 34.4 %slice-start = ((s8[4259840]{0:T(1024)(128)(4,1)}), s8[65536]{0:T(1024)(128)(4,1)S(1)}, s32[]{:S(2)}) async-start(s8[4259840]{0:T(1024)(128)(4,1)} %bitcast.58), calls=%async_computation.5 | async-start | bytes 131072
  239.6 42.6 %all-to-all-start.1 = ((bf16[1024,8,96]{0,2,1:T(8,128)(2,1)}), bf16[1024,8,96]{0,2,1:T(8,128)(2,1)}, u32[]{:S(2)}, u32[]{:S(2)}) async-start(bf16[1024,8,96]{0,2,1:T(8,128)(2,1)} %bitcast.18), calls=%async_computation.2 | async-start | bytes 3145728 | tf_op jit(solution)/shard_map/all_to_all | solution.py:91
  245.3 28.8 %slice-start.1 = ((s8[4259840]{0:T(1024)(128)(4,1)}), s8[4194304]{0:T(1024)(128)(4,1)S(1)}, s32[]{:S(2)}) async-start(s8[4259840]{0:T(1024)(128)(4,1)} %bitcast.58), calls=%async_computation.6 | async-start | bytes 8388608
  245.3 28.8 %copy-start.8 = (bf16[1,1024,1024]{2,1,0:T(8,128)(2,1)S(1)}, bf16[1,1024,1024]{2,1,0:T(8,128)(2,1)}, u32[]{:S(2)}) copy-start(bf16[1,1024,1024]{2,1,0:T(8,128)(2,1)} %param.13) | copy-start | bytes 6291460
  245.3 28.8 %copy-start.9 = (f32[1024]{0:T(1024)S(1)}, f32[1024]{0:T(1024)}, u32[]{:S(2)}) copy-start(f32[1024]{0:T(1024)} %param.14) | copy-start | bytes 12292
  282.2 12.1 %copy-start.1 = (bf16[1,256,4096]{2,1,0:T(8,128)(2,1)S(1)}, bf16[1,256,4096]{2,1,0:T(8,128)(2,1)}, u32[]{:S(2)}) copy-start(bf16[1,256,4096]{2,1,0:T(8,128)(2,1)} %param.21) | copy-start | bytes 6291460
Sparse Core Ops, SparseCore 0:
  79.5 45.3 all-gather.1
  139.1 97.1 reduce-scatter.1
where the time goes:
time: 302 us; the launch traced here: 301 us
  waiting for transfers between devices  127 us (42%)
  other arithmetic  52.6 us (17%)
  blocking collectives  50.1 us (17%)
  local copies, waits for them, and re-layouts  27.9 us (9%)
  matrix products  20.1 us (7%)
  between operations  14.3 us (5%)
  starting transfers between devices  9.46 us (3%)
    reduce_scatter x1, waiting for transfers between devices, shards(): lax.psum_scatter(lax.dot_general(w_down, flat_hidden, (((0,), (1,)), ((),...  78.7 us
    all_gather x1, waiting for transfers between devices, shards(): expand_arrived = lax.all_gather(arrived, 'tp', axis=1, tiled=True)  45.3 us
    all_to_all x1, blocking collectives, shards(): lax.all_to_all(mine, 'ep', split_axis=0, concat_axis=0, tiled=True)  44.2 us
    another operation x1, other arithmetic, shards(): jnp.stack(totals)  28.7 us
    gather x1, local copies, waits for them, and re-layouts, shards(): outgoing = jnp.take(padded_b, source, axis=0).reshape(experts, slots, D)  13.9 us
    dot_general x1, matrix products, shards(): jnp.dot(pooled, pool_weight[0], preferred_element_type=jnp.float32)  6.54 us
    dot_general x1, matrix products, shards(): lax.dot_general(w_down, flat_hidden, (((0,), (1,)), ((), ())), preferred_...  6.38 us
    reduce_sum x1, other arithmetic, shards(): moe_out = jnp.sum(weighted, axis=2).T.astype(jnp.bfloat16)  6.33 us
  transfers between devices with their start and end apart: 4, of which 4 were waited for; matrix products, arithmetic and copies ran while one was open for 14% of the time, Pallas kernels for 0%

commit v1 on v0

--- a/solution.py
+++ b/solution.py
@@ -1,6 +1,10 @@
+import functools
+
 import jax
 import jax.numpy as jnp
 from jax import lax
+from jax.experimental import pallas as pl
+from jax.experimental.pallas import tpu as pltpu
 from jax.sharding import PartitionSpec as P
 
 D = 4096
@@ -16,43 +20,418 @@
     return lax.ppermute(value, axis, [(source, source + steps) for source in range(first, last)])
 
 
-def shards(
-    mixer_in,
-    mixer_gain,
-    pool_weight,
-    pool_scale,
-    moe_in,
-    moe_gain,
-    route_expert,
-    route_weight,
-    gate_weight,
-    up_weight,
-    down_weight,
+GROUPS = 4
+MESH = pl.DeviceIdType.MESH
+
+
+def expert_kernel(
+    cap,
+    out_ref,
+    wrow_ref,
+    gate_hbm,
+    up_hbm,
+    down_hbm,
+    fin_ref,
+    xbuf,
+    wbuf,
+    wcol,
+    w_gate,
+    w_up,
+    w_down,
+    part_out,
+    part_in,
+    sums,
+    first_in,
+    second_in,
+    local_sem,
+    wsend,
+    wrecv,
+    zsend,
+    zrecv,
+    csend,
+    crecv,
+    psend,
+    precv,
+    fsend,
+    frecv,
 ):
-    rows = mixer_in.shape[0]
-    feats = mixer_in.astype(jnp.float32)
-    squares = lax.psum(jnp.sum(feats * feats, axis=1), "tp")
-    normed_a = (feats * lax.rsqrt(squares[:, None] / D + EPS) * mixer_gain).astype(jnp.bfloat16)
-    reach = WINDOW_MAX - 1
-    before = passed_along(normed_a[rows - reach :], "ep", 1)
-    extended = jnp.concatenate([before, normed_a], axis=0).astype(jnp.float32)
-    running = jnp.zeros((rows, normed_a.shape[1]), jnp.float32)
-    totals = []
-    for offset in range(WINDOW_MAX):
-        running = running + lax.slice_in_dim(
-            extended, reach - offset, reach - offset + rows, axis=0
+    ep, tp = lax.axis_index("ep"), lax.axis_index("tp")
+    z, y = ep // 2, ep % 2
+    x, c = tp // 2, tp % 2
+    width = out_ref.shape[1]
+    pair = 2 * cap
+
+    def dev(zz, yy, xx, cc):
+        return (zz * 2 + yy, xx * 2 + cc)
+
+    core_peer = dev(z, y, x, 1 - c)
+    x_peer = dev(z, y, 1 - x, c)
+    y_peer = dev(z, 1 - y, x, c)
+
+    loads = [
+        pltpu.make_async_copy(gate_hbm, w_gate, local_sem.at[0]),
+        pltpu.make_async_copy(up_hbm, w_up, local_sem.at[1]),
+        pltpu.make_async_copy(down_hbm, w_down, local_sem.at[2]),
+    ]
+    for load in loads:
+        load.start()
+
+    barrier = pltpu.get_barrier_semaphore()
+    peers = [core_peer, x_peer, y_peer]
+    for dz in range(GROUPS):
+        for other in range(2):
+            if dz or other:
+                peer = dev(lax.rem(z + dz, GROUPS), lax.rem(y + other, 2), x, c)
+                if not (dz == 0 and other == 1):
+                    peers.append(peer)
+    for peer in peers:
+        pl.semaphore_signal(barrier, inc=1, device_id=peer, device_id_type=MESH)
+    pl.semaphore_wait(barrier, len(peers))
+
+    def remote(src, dst, send, recv, peer):
+        copy = pltpu.make_async_remote_copy(
+            src_ref=src,
+            dst_ref=dst,
+            send_sem=send,
+            recv_sem=recv,
+            device_id=peer,
+            device_id_type=MESH,
         )
-        if offset > 0 and offset + 1 & offset == 0:
-            totals.append(running)
-    group = lax.axis_index("tp")
-    window_sum = lax.dynamic_index_in_dim(jnp.stack(totals), group, 0, keepdims=False)
-    span = jnp.left_shift(jnp.int32(2), group)
-    position = lax.axis_index("ep") * rows + jnp.arange(rows, dtype=jnp.int32)
-    count = jnp.minimum(position + 1, span).astype(jnp.float32)[:, None]
-    pooled = (window_sum / count - extended[reach:]).astype(jnp.bfloat16)
-    mixer_out = (
-        jnp.dot(pooled, pool_weight[0], preferred_element_type=jnp.float32) * pool_scale
+        return copy
+
+    def source_rows(zz, yy):
+        return pl.ds(pl.multiple_of((zz * 2 + yy) * cap, cap), cap)
+
+    def group_rows(g):
+        return pl.ds(pl.multiple_of(g * cap, cap), cap)
+
+    started = []
+
+    def go(copy):
+        copy.start()
+        started.append(copy)
+        return copy
+
+    zcopies = [None]
+    for dz in range(1, GROUPS):
+        g = lax.rem(z + dz, GROUPS)
+        zcopies.append(
+            go(
+                remote(
+                    out_ref.at[group_rows(g), :],
+                    xbuf.at[tp, source_rows(z, y), :],
+                    zsend.at[dz],
+                    zrecv.at[dz],
+                    dev(g, y, x, c),
+                )
+            )
+        )
+    keep = pltpu.make_async_copy(
+        out_ref.at[group_rows(z), :], xbuf.at[tp, source_rows(z, y), :], local_sem.at[3]
+    )
+    keep.start()
+    keep_w = pltpu.make_async_copy(wrow_ref.at[z], wbuf.at[ep], local_sem.at[4])
+    keep_w.start()
+    wcopies = []
+    for dz in range(GROUPS):
+        for other in range(2):
+            if dz or other:
+                g = lax.rem(z + dz, GROUPS)
+                wcopies.append(
+                    go(
+                        remote(
+                            wrow_ref.at[g],
+                            wbuf.at[ep],
+                            wsend.at[dz * 2 + other],
+                            wrecv.at[dz * 2 + other],
+                            dev(g, lax.rem(y + other, 2), x, c),
+                        )
+                    )
+                )
+
+    xq = (1 - x) * 2 + c
+    piece = {}
+
+    def share(name, index, k, quarter, yy, peer):
+        rows = source_rows(lax.rem(z + GROUPS - k, GROUPS), yy)
+        ref = xbuf.at[quarter, rows, :]
+        slot = index * GROUPS + k
+        piece[name, k] = go(remote(ref, ref, csend.at[slot], crecv.at[slot], peer))
+
+    def own(k):
+        if k:
+            zcopies[k].wait_recv()
+        else:
+            keep.wait()
+        share("x", 0, k, tp, y, x_peer)
+        share("y", 1, k, tp, y, y_peer)
+        share("c", 2, k, tp, y, core_peer)
+
+    def relay(k):
+        piece["x", k].wait_recv()
+        if k % 2 == 0:
+            share("d", 3, k, xq, y, y_peer)
+        share("xc", 4, k, xq, y, core_peer)
+        piece["y", k].wait_recv()
+        if k % 2 == 1:
+            share("d", 3, k, tp, 1 - y, x_peer)
+        share("yc", 5, k, tp, 1 - y, core_peer)
+
+    def diagonal(k):
+        piece["d", k].wait_recv()
+        share("dc", 6, k, xq, 1 - y, core_peer)
+
+    def complete(k):
+        for name in ("c", "xc", "yc", "dc"):
+            piece[name, k].wait_recv()
+
+    def chunk_rows(k):
+        return pl.ds(pl.multiple_of(lax.rem(z + GROUPS - k, GROUPS) * pair, pair), pair)
+
+    def columns(xx, cc):
+        return pl.ds(pl.multiple_of((xx * 2 + cc) * width, width), width)
+
+    hidden = {}
+    away = {}
+
+    def expand(k):
+        rows = chunk_rows(k)
+        gate = jnp.zeros((pair, w_gate.shape[1]), jnp.float32)
+        upper = gate
+        for q in range(xbuf.shape[0]):
+            block = xbuf[q, rows, :]
+            gate += jnp.dot(
+                block, w_gate[q * width : (q + 1) * width, :], preferred_element_type=jnp.float32
+            )
+            upper += jnp.dot(
+                block, w_up[q * width : (q + 1) * width, :], preferred_element_type=jnp.float32
+            )
+        scale = wcol[rows, :]
+        scale = jnp.concatenate([scale] * (w_gate.shape[1] // scale.shape[1]), axis=1)
+        value = (gate / (1.0 + jnp.exp(-gate))) * upper * scale
+        hidden[k] = value.astype(jnp.bfloat16)
+        for xx in range(2):
+            part_out[k, xx] = jnp.dot(
+                hidden[k], w_down[:, columns(xx, 1 - c)], preferred_element_type=jnp.float32
+            ).astype(jnp.bfloat16)
+            slot = k * 2 + xx
+            away[k, xx] = go(
+                remote(
+                    part_out.at[k, xx], part_in.at[k, xx], psend.at[slot], precv.at[slot], core_peer
+                )
+            )
+
+    hop = {}
+
+    def first_hop(k):
+        for xx in range(2):
+            mine = jnp.dot(
+                hidden[k], w_down[:, columns(xx, c)], preferred_element_type=jnp.float32
+            )
+            away[k, xx].wait_recv()
+            sums[k, xx] = (mine + part_in[k, xx].astype(jnp.float32)).astype(jnp.bfloat16)
+        if k % 2 == 0:
+            slot = k * 4
+            hop[k, 0] = go(
+                remote(
+                    sums.at[k, 1 - x], first_in.at[k], fsend.at[slot], frecv.at[slot], x_peer
+                )
+            )
+        else:
+            for xx in range(2):
+                slot = k * 4 + xx
+                hop[k, xx] = go(
+                    remote(
+                        sums.at[k, xx, group_rows(1 - y), :],
+                        first_in.at[k, xx * cap : (xx + 1) * cap, :],
+                        fsend.at[slot],
+                        frecv.at[slot],
+                        y_peer,
+                    )
+                )
+
+    def second_hop(k):
+        slot = k * 4 + 2
+        if k % 2 == 0:
+            hop[k, 0].wait_recv()
+            total = sums[k, x].astype(jnp.float32) + first_in[k].astype(jnp.float32)
+            sums[k, x] = total.astype(jnp.bfloat16)
+            hop[k, 2] = go(
+                remote(
+                    sums.at[k, x, group_rows(1 - y), :],
+                    second_in.at[k],
+                    fsend.at[slot],
+                    frecv.at[slot],
+                    y_peer,
+                )
+            )
+        else:
+            for xx in range(2):
+                hop[k, xx].wait_recv()
+                total = sums[k, xx, group_rows(y), :].astype(jnp.float32) + first_in[
+                    k, xx * cap : (xx + 1) * cap, :
+                ].astype(jnp.float32)
+                sums[k, xx, group_rows(y), :] = total.astype(jnp.bfloat16)
+            hop[k, 2] = go(
+                remote(
+                    sums.at[k, 1 - x, group_rows(y), :],
+                    second_in.at[k],
+                    fsend.at[slot],
+                    frecv.at[slot],
+                    x_peer,
+                )
+            )
+
+    home = {}
+
+    def homeward(k):
+        hop[k, 2].wait_recv()
+        total = sums[k, x, group_rows(y), :].astype(jnp.float32) + second_in[k].astype(jnp.float32)
+        if k == 0:
+            fin_ref[group_rows(z), :] = total.astype(jnp.bfloat16)
+            return
+        sums[k, x, group_rows(y), :] = total.astype(jnp.bfloat16)
+        slot = k * 4 + 3
+        home[k] = go(
+            remote(
+                sums.at[k, x, group_rows(y), :],
+                fin_ref.at[group_rows(z), :],
+                fsend.at[slot],
+                frecv.at[slot],
+                dev(lax.rem(z + GROUPS - k, GROUPS), y, x, c),
+            )
+        )
+
+    own(0)
+    own(1)
+    relay(0)
+    own(2)
+    relay(1)
+    diagonal(0)
+    keep_w.wait()
+    for copy in wcopies:
+        copy.wait_recv()
+    for source in range(wbuf.shape[0]):
+        line = jnp.where(y == 0, wbuf[source, 0:1, :], wbuf[source, 1:2, :])
+        wcol[source * cap : (source + 1) * cap, :] = jnp.broadcast_to(line, (128, 128)).T[:cap]
+    for load in loads:
+        load.wait()
+    complete(0)
+    expand(0)
+    own(3)
+    relay(2)
+    diagonal(1)
+    first_hop(0)
+    complete(1)
+    expand(1)
+    relay(3)
+    diagonal(2)
+    first_hop(1)
+    complete(2)
+    expand(2)
+    diagonal(3)
+    second_hop(0)
+    first_hop(2)
+    complete(3)
+    expand(3)
+    second_hop(1)
+    first_hop(3)
+    homeward(0)
+    homeward(1)
+    second_hop(2)
+    second_hop(3)
+    homeward(2)
+    homeward(3)
+    for k in range(1, GROUPS):
+        home[k].wait_recv()
+    for copy in started:
+        copy.wait_send()
+
+
+def paired_experts(
+    moe_in, moe_gain, route_expert, route_weight, gate_weight, up_weight, down_weight
+):
+    tokens = moe_in.shape[0]
+    n_ep, n_tp = lax.axis_size("ep"), lax.axis_size("tp")
+    cap = 3 * tokens // n_ep
+    width = moe_in.shape[1] // n_tp
+    units = gate_weight.shape[2]
+    tp = lax.axis_index("tp")
+    slots = GROUPS * cap
+    group = route_expert[:, 0] // 2
+    lanes = jnp.arange(GROUPS, dtype=jnp.int32)
+    member = group[:, None] == lanes[None, :]
+    order = jnp.arange(tokens, dtype=jnp.int32)
+    before = (order[:, None] > order[None, :]).astype(jnp.bfloat16)
+    ahead = jnp.dot(before, member.astype(jnp.bfloat16), preferred_element_type=jnp.float32)
+    rank = jnp.sum(jnp.where(member, ahead, 0.0), axis=1).astype(jnp.int32)
+    slot = group * cap + rank
+    select = (jnp.arange(slots, dtype=jnp.int32)[:, None] == slot[None, :]).astype(jnp.bfloat16)
+    feats = moe_in.astype(jnp.float32)
+    factor = lax.rsqrt(jnp.mean(feats * feats, axis=1, keepdims=True) + EPS)
+    mine = lax.dynamic_slice_in_dim(moe_in, tp * width, width, 1).astype(jnp.float32)
+    gain = lax.dynamic_slice_in_dim(moe_gain, tp * width, width, 0)
+    normed = (mine * factor * gain).astype(jnp.bfloat16)
+    outgoing = jnp.dot(select, normed, preferred_element_type=jnp.float32).astype(jnp.bfloat16)
+    lane = jnp.arange(128, dtype=jnp.int32)
+    wide = (rank[:, None] == lane[None, :]).astype(jnp.float32)
+    by_expert = jnp.sum(
+        jnp.where(
+            (route_expert % 2)[:, :, None] == jnp.arange(8, dtype=jnp.int32)[None, None, :],
+            route_weight[:, :, None],
+            0.0,
+        ),
+        axis=1,
+    )
+    spread = (member[:, :, None] * by_expert[:, None, :]).reshape(tokens, GROUPS * 8)
+    wrow = jnp.dot(
+        spread.T, wide, precision=lax.Precision.HIGHEST, preferred_element_type=jnp.float32
+    ).reshape(GROUPS, 8, 128)
+    vmem = pl.BlockSpec(memory_space=pltpu.VMEM)
+    hbm = pl.BlockSpec(memory_space=pl.ANY)
+    dma = pltpu.SemaphoreType.DMA
+    model = moe_in.shape[1]
+    fin = pl.pallas_call(
+        functools.partial(expert_kernel, cap),
+        out_shape=jax.ShapeDtypeStruct((slots, width), jnp.bfloat16),
+        in_specs=[vmem, vmem, hbm, hbm, hbm],
+        out_specs=vmem,
+        scratch_shapes=[
+            pltpu.VMEM((n_tp, n_ep * cap, width), jnp.bfloat16),
+            pltpu.VMEM((n_ep, 8, 128), jnp.float32),
+            pltpu.VMEM((n_ep * cap, 128), jnp.float32),
+            pltpu.VMEM((model, units), jnp.bfloat16),
+            pltpu.VMEM((model, units), jnp.bfloat16),
+            pltpu.VMEM((units, model), jnp.bfloat16),
+            pltpu.VMEM((GROUPS, 2, 2 * cap, width), jnp.bfloat16),
+            pltpu.VMEM((GROUPS, 2, 2 * cap, width), jnp.bfloat16),
+            pltpu.VMEM((GROUPS, 2, 2 * cap, width), jnp.bfloat16),
+            pltpu.VMEM((GROUPS, 2 * cap, width), jnp.bfloat16),
+            pltpu.VMEM((GROUPS, cap, width), jnp.bfloat16),
+            dma((5,)),
+            dma((8,)),
+            dma((8,)),
+            dma((4,)),
+            dma((4,)),
+            dma((28,)),
+            dma((28,)),
+            dma((8,)),
+            dma((8,)),
+            dma((16,)),
+            dma((16,)),
+        ],
+        compiler_params=pltpu.CompilerParams(
+            collective_id=0, has_side_effects=True, vmem_limit_bytes=56 * 1024 * 1024
+        ),
+    )(outgoing, wrow, gate_weight[0], up_weight[0], down_weight[0])
+    return lax.dot_general(
+        select, fin, (((0,), (0,)), ((), ())), preferred_element_type=jnp.float32
     ).astype(jnp.bfloat16)
+
+
+def any_experts(
+    moe_in, moe_gain, route_expert, route_weight, gate_weight, up_weight, down_weight
+):
     tokens = moe_in.shape[0]
     feats_b = moe_in.astype(jnp.float32)
     normed_b = (
@@ -94,6 +473,51 @@
     picked = jnp.take(back.reshape(columns, experts * slots), slot_index, axis=1)
     weighted = picked.astype(jnp.float32).reshape(columns, tokens, 2) * route_weight[None, :, :]
     moe_out = jnp.sum(weighted, axis=2).T.astype(jnp.bfloat16)
+    return moe_out
+
+
+def shards(
+    mixer_in,
+    mixer_gain,
+    pool_weight,
+    pool_scale,
+    moe_in,
+    moe_gain,
+    route_expert,
+    route_weight,
+    gate_weight,
+    up_weight,
+    down_weight,
+):
+    rows = mixer_in.shape[0]
+    feats = mixer_in.astype(jnp.float32)
+    squares = lax.psum(jnp.sum(feats * feats, axis=1), "tp")
+    normed_a = (feats * lax.rsqrt(squares[:, None] / D + EPS) * mixer_gain).astype(jnp.bfloat16)
+    reach = WINDOW_MAX - 1
+    before = passed_along(normed_a[rows - reach :], "ep", 1)
+    extended = jnp.concatenate([before, normed_a], axis=0).astype(jnp.float32)
+    running = jnp.zeros((rows, normed_a.shape[1]), jnp.float32)
+    totals = []
+    for offset in range(WINDOW_MAX):
+        running = running + lax.slice_in_dim(
+            extended, reach - offset, reach - offset + rows, axis=0
+        )
+        if offset > 0 and offset + 1 & offset == 0:
+            totals.append(running)
+    group = lax.axis_index("tp")
+    window_sum = lax.dynamic_index_in_dim(jnp.stack(totals), group, 0, keepdims=False)
+    span = jnp.left_shift(jnp.int32(2), group)
+    position = lax.axis_index("ep") * rows + jnp.arange(rows, dtype=jnp.int32)
+    count = jnp.minimum(position + 1, span).astype(jnp.float32)[:, None]
+    pooled = (window_sum / count - extended[reach:]).astype(jnp.bfloat16)
+    mixer_out = (
+        jnp.dot(pooled, pool_weight[0], preferred_element_type=jnp.float32) * pool_scale
+    ).astype(jnp.bfloat16)
+    paired = lax.axis_size("ep") == 2 * GROUPS and lax.axis_size("tp") == 4
+    experts_of = paired_experts if paired else any_experts
+    moe_out = experts_of(
+        moe_in, moe_gain, route_expert, route_weight, gate_weight, up_weight, down_weight
+    )
     return (mixer_out, moe_out)
 
 

time: 302 us -> 129 us (0.43)
  waiting for transfers between devices: 127 us -> 0.01 us
  Pallas kernels: 0 us -> 85.6 us
  blocking collectives: 50.1 us -> 8.38 us
  other arithmetic: 52.6 us -> 16.2 us
  local copies, waits for them, and re-layouts: 27.9 us -> 2.04 us
  between operations: 14.3 us -> 0.78 us
  matrix products: 20.1 us -> 12.4 us
  starting transfers between devices: 9.46 us -> 3.43 us
    pallas_call x0 -> x1, Pallas kernels: none -> 85.6 us  [paired_experts(): pl.pallas_call(functools.partial(expert_kernel, cap), out_shape=jax.Shape...]
    reduce_scatter x1 -> x0, waiting for transfers between devices: 78.7 us -> none  [shards(): lax.psum_scatter(lax.dot_general(w_down, flat_hidden, (((0,), (1,)), ((),...]
    all_gather x1 -> x0, waiting for transfers between devices: 45.3 us -> none  [shards(): expand_arrived = lax.all_gather(arrived, 'tp', axis=1, tiled=True)]
    all_to_all x1 -> x0, blocking collectives: 44.2 us -> none  [shards(): lax.all_to_all(mine, 'ep', split_axis=0, concat_axis=0, tiled=True)]
    another operation x1, other arithmetic: 28.7 us -> 7.5 us  [shards(): jnp.stack(totals)]
    gather x3 -> x0, local copies, waits for them, and re-layouts: 19.6 us -> none  [the longest x1 13.9 us: shards(): outgoing = jnp.take(padded_b, source, axis=0).reshape(experts, slots, D)]
    dot_general x3 -> x4, matrix products: 13.6 us -> 5.89 us  [the longest x1 2.43 us: paired_experts(): jnp.dot(select, normed, preferred_element_type=jnp.float32)]
    reduce_sum x3 -> x2, other arithmetic: 8.51 us -> 2.09 us  [the longest x1 2.09 us: paired_experts(): factor = lax.rsqrt(jnp.mean(feats * feats, axis=1, keepdims=True) + EPS)]
  transfers between devices with their start and end apart: 4 -> 1, of which waited for: 4 -> 0; matrix products, arithmetic and copies ran while one was open for 14% -> 7% of each run, Pallas kernels for 0% -> 66%
where the time goes in v1:
time: 129 us
  Pallas kernels  85.6 us (66%)
  other arithmetic  16.2 us (13%)
  matrix products  12.4 us (10%)
  blocking collectives  8.38 us (6%)
  starting transfers between devices  3.43 us (3%)
  local copies, waits for them, and re-layouts  2.04 us (2%)
    pallas_call x1, Pallas kernels, paired_experts(): pl.pallas_call(functools.partial(expert_kernel, cap), out_shape=jax.Shape...  85.6 us
    psum x1, blocking collectives, shards(): squares = lax.psum(jnp.sum(feats * feats, axis=1), 'tp')  8.38 us
    another operation x1, other arithmetic, shards(): jnp.stack(totals)  7.5 us
    dot_general x1, matrix products, shards(): jnp.dot(pooled, pool_weight[0], preferred_element_type=jnp.float32)  6.53 us
    ppermute x1, starting transfers between devices, passed_along(): lax.ppermute(value, axis, [(source, source + steps) for source in range(f...  3.43 us
  transfers between devices with their start and end apart: 1, of which 0 were waited for; matrix products, arithmetic and copies ran while one was open for 7% of the time, Pallas kernels for 66%

profile of v1, /device:TPU:0, one launch (start us, length us, event | category | flops | bytes accessed | tf_op | source)
XLA Modules:
  0.0 128.9 jit_solution(8660573466027234704)
XLA Ops:
  0.6 0.0 copy-start
  0.6 0.0 copy-start.2
  0.7 0.0 copy-start.3
  0.7 2.2 %fusion = f32[1024]{0:T(1024)S(1)} fusion(bf16[1024,1024]{1,0:T(8,128)(2,1)} %param.11), kind=kLoop, calls=%fused_computation.6 | loop fusion | flops 3144704 | bytes 2101248 | tf_op jit(solution)/shard_map/reduce_sum | solution.py:494
  2.9 8.4 %psum.7 = f32[1024]{0:T(1024)S(1)} all-reduce(f32[1024]{0:T(1024)S(1)} %fusion), channel_id=1, replica_groups=mesh['ep'=8,'tp'=4] {'tp'}, use_global_device_ids=true, to_apply=%region_1.0 | all-reduce | flops 1024 | bytes 8192 | tf_op jit(solution)/shard_map/psum | solution.py:494
  11.3 2.1 %fusion.2 = bf16[1024,1024]{1,0:T(8,128)(2,1)S(1)} fusion(bf16[1024,1024]{1,0:T(8,128)(2,1)} %param.11, f32[1024]{0:T(1024)} %param.12, f32[1024]{0:T(1024)S(1)} %add_rsqrt_fusion), kind=kLoop, calls=%fused_computation.8 | loop fusion | flops 4194304 | bytes 4202496 | tf_op jit(solution)/shard_map/convert_element_type | solution.py:495
  13.4 0.0 copy-start.1
  13.4 1.3 %copy-done.1 = bf16[1024,1024]{1,0:T(8,128)(2,1)} copy-done((bf16[1024,1024]{1,0:T(8,128)(2,1)}, bf16[1024,1024]{1,0:T(8,128)(2,1)S(1)}, u32[]{:S(2)}) %copy-start.1) | copy-done | bytes 2097176
  14.7 3.4 %collective-permute-start = (bf16[15,1024]{1,0:T(8,128)(2,1)S(1)}, bf16[15,1024]{1,0:T(8,128)(2,1)S(1)}, u32[]{:S(2)}, u32[]{:S(2)}) collective-permute-start(bf16[15,1024]{1,0:T(8,128)(2,1)S(1)} %slice.73), channel_id=1, source_target_pairs={{0,4},{4,8},{8,12},{12,16},{16,20},{20,24},{24,28},{1,5},{5,9},{9,... | collective-permute-start | bytes 92168 | tf_op jit(solution)/shard_map/ppermute | solution.py:20
  18.2 0.0 copy-done.2
  18.2 0.2 fusion.14
  18.5 2.1 %multiply_reduce_fusion = f32[256]{0:T(256)S(1)} fusion(bf16[256,4096]{1,0:T(8,128)(2,1)} %param.15), kind=kLoop, calls=%fused_computation.31 | loop fusion | flops 3145472 | bytes 2098176 | tf_op jit(solution)/shard_map/reduce_sum | solution.py:371
  20.6 0.7 dynamic_slice.12
  21.3 0.0 copy-done.3
  21.3 2.4 %convolution_convert_fusion.out_ref = bf16[384,1024]{1,0:T(8,128)(2,1)} fusion(f32[1024]{0:T(1024)S(1)} %dynamic_slice.12, f32[256]{0:T(256)S(1)} %add_rsqrt_fusion.1, bf16[256,4096]{1,0:T(8,128)(2,1)} %param.15, s32[]{:T(128)S(6)} %select_n.39, s32[256]{0:T(256)S(1)} %multiply_add_fusion), kind=kOutput, calls=%fused_computation.36 | convolution fusion | flops 202866688 | bytes 1316868 | tf_op jit(solution)/shard_map/dot_general | solution.py:375
  23.7 0.9 fusion.21.wrow_ref
  24.6 85.6 %shard_map.122 = bf16[384,1024]{1,0:T(8,128)(2,1)} custom-call(bf16[384,1024]{1,0:T(8,128)(2,1)} %convolution_convert_fusion.out_ref, f32[4,8,128]{2,1,0:T(8,128)} %fusion.21.wrow_ref, bf16[4096,256]{1,0:T(8,128)(2,1)} %bitcast.36, bf16[4096,256]{1,0:T(8,128)(2,1)} %bitcast.37, bf16[256,4096]{1,0:T(8,128)(2,1)} %bitcast.38), custom_call_target="tpu_custom_call" | custom-call | tf_op jit(solution)/shard_map/pallas_call | solution.py:394
  110.2 2.4 %convolution_convert_fusion.1 = bf16[256,1024]{1,0:T(8,128)(2,1)} fusion(bf16[384,1024]{1,0:T(8,128)(2,1)} %shard_map.122, s32[256]{0:T(256)S(1)} %multiply_add_fusion), kind=kOutput, calls=%fused_computation.38 | convolution fusion | flops 201687040 | bytes 1311744 | tf_op jit(solution)/shard_map/dot_general | solution.py:427
  112.6 0.0 collective-permute-done
  112.6 2.2 %maximum_convert_fusion = f32[1039,1024]{1,0:T(8,128)S(1)} fusion(bf16[1024,1024]{1,0:T(8,128)(2,1)} %copy-done.1, bf16[15,1024]{1,0:T(8,128)(2,1)S(1)} %collective-permute-done), kind=kLoop, calls=%fused_computation.34 | loop fusion | flops 4255744 | bytes 6383616 | tf_op jit(solution)/shard_map/convert_element_type | solution.py:498
  114.9 0.0 copy-start.4
  114.9 7.5 %fusion.9 = (f32[1,1024,1024]{2,1,0:T(8,128)S(1)}, f32[1024,1024]{1,0:T(8,128)}, f32[1024,1024]{1,0:T(8,128)}, f32[1,1024,1024]{2,1,0:T(8,128)}) fusion(f32[1039,1024]{1,0:T(8,128)S(1)} %maximum_convert_fusion), kind=kLoop, calls=%fused_computation.16 | loop fusion | flops 15728640 | bytes 83886080 | tf_op jit(solution)/shard_map/stack | solution.py:508
  122.4 0.0 copy-done
  122.4 6.5 %multiply_convert_fusion = bf16[1024,1024]{1,0:T(8,128)(2,1)} fusion(bf16[1,1024,1024]{2,1,0:T(8,128)(2,1)S(1)} %copy-done, f32[1024]{0:T(1024)S(1)} %copy-done.4, s32[]{:T(128)S(6)} %select_n.35, f32[1,1024,1024]{2,1,0:T(8,128)S(1)} %get-tuple-element.2, f32[1,1024,1024]{2,1,0:T(8,128)} %bitcast.34, f32[1,1024,1024]{2,1,0:T(8,128)} %bitcast.35, ...), kind=kOutput, calls=%fused_computation.32 | convolution fusion | flops 2155872256 | bytes 25174020 | tf_op jit(solution)/shard_map/dot_general | solution.py:514
  (11 shorter events, 0.1 us)
Async XLA Ops:
  0.6 121.7 %copy-start = (bf16[1,1024,1024]{2,1,0:T(8,128)(2,1)S(1)}, bf16[1,1024,1024]{2,1,0:T(8,128)(2,1)}, u32[]{:S(2)}) copy-start(bf16[1,1024,1024]{2,1,0:T(8,128)(2,1)} %param.13) | copy-start | bytes 6291460
  0.6 17.5 %copy-start.2 = (s32[256,2]{0,1:T(2,128)S(1)}, s32[256,2]{0,1:T(2,128)}, u32[]{:S(2)}) copy-start(s32[256,2]{0,1:T(2,128)} %param.17) | copy-start | bytes 6148
  0.7 20.6 %copy-start.3 = (f32[256,2]{0,1:T(2,128)S(1)}, f32[256,2]{0,1:T(2,128)}, u32[]{:S(2)}) copy-start(f32[256,2]{0,1:T(2,128)} %param.18) | copy-start | bytes 6148
  13.4 1.3 %copy-start.1 = (bf16[1024,1024]{1,0:T(8,128)(2,1)}, bf16[1024,1024]{1,0:T(8,128)(2,1)S(1)}, u32[]{:S(2)}) copy-start(bf16[1024,1024]{1,0:T(8,128)(2,1)S(1)} %fusion.2) | copy-start | bytes 6291460
  14.7 97.9 %collective-permute-start = (bf16[15,1024]{1,0:T(8,128)(2,1)S(1)}, bf16[15,1024]{1,0:T(8,128)(2,1)S(1)}, u32[]{:S(2)}, u32[]{:S(2)}) collective-permute-start(bf16[15,1024]{1,0:T(8,128)(2,1)S(1)} %slice.73), channel_id=1, source_target_pairs={{0,4},{4,8},{8,12},{12,16},{16,20},{20,24},{24,28},{1,5},{5,9},{9,... | collective-permute-start | bytes 92168 | tf_op jit(solution)/shard_map/ppermute | solution.py:20
  114.9 7.5 %copy-start.4 = (f32[1024]{0:T(1024)S(1)}, f32[1024]{0:T(1024)}, u32[]{:S(2)}) copy-start(f32[1024]{0:T(1024)} %param.14) | copy-start | bytes 12292

commit v2 on v1

--- a/solution.py
+++ b/solution.py
@@ -31,7 +31,12 @@
     gate_hbm,
     up_hbm,
     down_hbm,
+    mixer_hbm,
+    gain_ref,
+    pool_hbm,
+    scale_ref,
     fin_ref,
+    mixed_ref,
     xbuf,
     wbuf,
     wcol,
@@ -54,6 +59,14 @@
     precv,
     fsend,
     frecv,
+    feats,
+    w_pool,
+    squares,
+    squares_in,
+    factors,
+    normed,
+    msend,
+    mrecv,
 ):
     ep, tp = lax.axis_index("ep"), lax.axis_index("tp")
     z, y = ep // 2, ep % 2
@@ -73,11 +86,16 @@
         pltpu.make_async_copy(up_hbm, w_up, local_sem.at[1]),
         pltpu.make_async_copy(down_hbm, w_down, local_sem.at[2]),
     ]
+    mixer_load = pltpu.make_async_copy(mixer_hbm, feats, local_sem.at[5])
+    pool_load = pltpu.make_async_copy(pool_hbm, w_pool, local_sem.at[6])
+    mixer_load.start()
     for load in loads:
         load.start()
+    pool_load.start()
 
     barrier = pltpu.get_barrier_semaphore()
-    peers = [core_peer, x_peer, y_peer]
+    cross_peer = dev(z, y, 1 - x, 1 - c)
+    peers = [core_peer, x_peer, y_peer, cross_peer]
     for dz in range(GROUPS):
         for other in range(2):
             if dz or other:
@@ -152,9 +170,12 @@
     xq = (1 - x) * 2 + c
     piece = {}
 
-    def share(name, index, k, quarter, yy, peer):
+    half = width // 2
+
+    def share(name, index, k, quarter, yy, peer, part=None):
         rows = source_rows(lax.rem(z + GROUPS - k, GROUPS), yy)
-        ref = xbuf.at[quarter, rows, :]
+        cols = slice(None) if part is None else pl.ds(part * half, half)
+        ref = xbuf.at[quarter, rows, cols]
         slot = index * GROUPS + k
         piece[name, k] = go(remote(ref, ref, csend.at[slot], crecv.at[slot], peer))
 
@@ -169,16 +190,15 @@
 
     def relay(k):
         piece["x", k].wait_recv()
-        if k % 2 == 0:
-            share("d", 3, k, xq, y, y_peer)
+        share("d0", 3, k, xq, y, y_peer, 0)
         share("xc", 4, k, xq, y, core_peer)
         piece["y", k].wait_recv()
-        if k % 2 == 1:
-            share("d", 3, k, tp, 1 - y, x_peer)
+        share("d1", 7, k, tp, 1 - y, x_peer, 1)
         share("yc", 5, k, tp, 1 - y, core_peer)
 
     def diagonal(k):
-        piece["d", k].wait_recv()
+        piece["d0", k].wait_recv()
+        piece["d1", k].wait_recv()
         share("dc", 6, k, xq, 1 - y, core_peer)
 
     def complete(k):
@@ -230,84 +250,173 @@
             )
             away[k, xx].wait_recv()
             sums[k, xx] = (mine + part_in[k, xx].astype(jnp.float32)).astype(jnp.bfloat16)
-        if k % 2 == 0:
-            slot = k * 4
-            hop[k, 0] = go(
+        hop[k, 0] = go(
+            remote(
+                sums.at[k, 1 - x, :, 0:half],
+                first_in.at[k, 0],
+                fsend.at[k * 6],
+                frecv.at[k * 6],
+                x_peer,
+            )
+        )
+        for xx in range(2):
+            hop[k, 1 + xx] = go(
                 remote(
-                    sums.at[k, 1 - x], first_in.at[k], fsend.at[slot], frecv.at[slot], x_peer
-                )
-            )
-        else:
-            for xx in range(2):
-                slot = k * 4 + xx
-                hop[k, xx] = go(
+                    sums.at[k, xx, group_rows(1 - y), half:width],
+                    first_in.at[k, 1, xx * cap : (xx + 1) * cap, :],
+                    fsend.at[k * 6 + 1 + xx],
+                    frecv.at[k * 6 + 1 + xx],
+                    y_peer,
+                )
+            )
+
+    def second_hop(k):
+        hop[k, 0].wait_recv()
+        total = sums[k, x, :, 0:half].astype(jnp.float32) + first_in[k, 0].astype(jnp.float32)
+        sums[k, x, :, 0:half] = total.astype(jnp.bfloat16)
+        hop[k, 3] = go(
+            remote(
+                sums.at[k, x, group_rows(1 - y), 0:half],
+                second_in.at[k, 0],
+                fsend.at[k * 6 + 3],
+                frecv.at[k * 6 + 3],
+                y_peer,
+            )
+        )
+        for xx in range(2):
+            hop[k, 1 + xx].wait_recv()
+            total = sums[k, xx, group_rows(y), half:width].astype(jnp.float32) + first_in[
+                k, 1, xx * cap : (xx + 1) * cap, :
+            ].astype(jnp.float32)
+            sums[k, xx, group_rows(y), half:width] = total.astype(jnp.bfloat16)
+        hop[k, 4] = go(
+            remote(
+                sums.at[k, 1 - x, group_rows(y), half:width],
+                second_in.at[k, 1],
+                fsend.at[k * 6 + 4],
+                frecv.at[k * 6 + 4],
+                x_peer,
+            )
+        )
+
+    home = {}
+
+    def homeward(k):
+        for part in range(2):
+            cols = slice(part * half, (part + 1) * half)
+            hop[k, 3 + part].wait_recv()
+            total = sums[k, x, group_rows(y), cols].astype(jnp.float32) + second_in[
+                k, part
+            ].astype(jnp.float32)
+            if k == 0:
+                fin_ref[group_rows(z), cols] = total.astype(jnp.bfloat16)
+            else:
+                sums[k, x, group_rows(y), cols] = total.astype(jnp.bfloat16)
+        if k:
+            home[k] = go(
+                remote(
+                    sums.at[k, x, group_rows(y), :],
+                    fin_ref.at[group_rows(z), :],
+                    fsend.at[k * 6 + 5],
+                    frecv.at[k * 6 + 5],
+                    dev(lax.rem(z + GROUPS - k, GROUPS), y, x, c),
+                )
+            )
+
+    rows, channels = feats.shape
+    tiles = rows // 128
+    reach = WINDOW_MAX
+
+    def tile_rows(i, start=0, count=128):
+        return pl.ds(pl.multiple_of(i * 128 + start, 16), count)
+
+    mixer_copies = []
+
+    def square_sums():
+        mixer_load.wait()
+
+        @pl.loop(0, tiles)
+        def _(i):
+            total = jnp.zeros((128, 128), jnp.float32)
+            for q in range(channels // 128):
+                value = feats[tile_rows(i), q * 128 : (q + 1) * 128].astype(jnp.float32)
+                total += value * value
+            squares[pl.ds(i, 1), :] = jnp.sum(total.T, axis=0, keepdims=True)
+
+        for index, peer in enumerate((core_peer, x_peer, cross_peer)):
+            mixer_copies.append(
+                go(
                     remote(
-                        sums.at[k, xx, group_rows(1 - y), :],
-                        first_in.at[k, xx * cap : (xx + 1) * cap, :],
-                        fsend.at[slot],
-                        frecv.at[slot],
-                        y_peer,
+                        squares, squares_in.at[index], msend.at[index], mrecv.at[index], peer
                     )
                 )
-
-    def second_hop(k):
-        slot = k * 4 + 2
-        if k % 2 == 0:
-            hop[k, 0].wait_recv()
-            total = sums[k, x].astype(jnp.float32) + first_in[k].astype(jnp.float32)
-            sums[k, x] = total.astype(jnp.bfloat16)
-            hop[k, 2] = go(
+            )
+
+    def normalize():
+        for copy in mixer_copies:
+            copy.wait_recv()
+        total = squares[...] + squares_in[0] + (squares_in[1] + squares_in[2])
+        factors[...] = lax.rsqrt(total / D + EPS)
+
+        @pl.loop(0, tiles)
+        def _(i):
+            factor = jnp.broadcast_to(factors[pl.ds(i, 1), :], (128, 128)).T
+            for q in range(channels // 128):
+                cols = slice(q * 128, (q + 1) * 128)
+                value = feats[tile_rows(i), cols].astype(jnp.float32) * factor * gain_ref[:, cols]
+                normed[tile_rows(i, reach), cols] = value.astype(jnp.bfloat16)
+
+        following = lax.rem(ep + 1, 2 * GROUPS)
+        mixer_copies.append(
+            go(
                 remote(
-                    sums.at[k, x, group_rows(1 - y), :],
-                    second_in.at[k],
-                    fsend.at[slot],
-                    frecv.at[slot],
-                    y_peer,
-                )
-            )
-        else:
-            for xx in range(2):
-                hop[k, xx].wait_recv()
-                total = sums[k, xx, group_rows(y), :].astype(jnp.float32) + first_in[
-                    k, xx * cap : (xx + 1) * cap, :
-                ].astype(jnp.float32)
-                sums[k, xx, group_rows(y), :] = total.astype(jnp.bfloat16)
-            hop[k, 2] = go(
-                remote(
-                    sums.at[k, 1 - x, group_rows(y), :],
-                    second_in.at[k],
-                    fsend.at[slot],
-                    frecv.at[slot],
-                    x_peer,
-                )
-            )
-
-    home = {}
-
-    def homeward(k):
-        hop[k, 2].wait_recv()
-        total = sums[k, x, group_rows(y), :].astype(jnp.float32) + second_in[k].astype(jnp.float32)
-        if k == 0:
-            fin_ref[group_rows(z), :] = total.astype(jnp.bfloat16)
-            return
-        sums[k, x, group_rows(y), :] = total.astype(jnp.bfloat16)
-        slot = k * 4 + 3
-        home[k] = go(
-            remote(
-                sums.at[k, x, group_rows(y), :],
-                fin_ref.at[group_rows(z), :],
-                fsend.at[slot],
-                frecv.at[slot],
-                dev(lax.rem(z + GROUPS - k, GROUPS), y, x, c),
+                    normed.at[rows : rows + reach, :],
+                    normed.at[0:reach, :],
+                    msend.at[3],
+                    mrecv.at[3],
+                    (following, tp),
+                )
             )
         )
 
+    def halo():
+        mixer_copies[3].wait_recv()
+        edge = normed[0:reach, :]
+        normed[0:reach, :] = jnp.where(ep == 0, jnp.zeros_like(edge), edge)
+        pool_load.wait()
+
+    def pool(first, last):
+        span = jnp.where(tp == 0, 2, jnp.where(tp == 1, 4, jnp.where(tp == 2, 8, 16)))
+
+        @pl.loop(first, last)
+        def _(i):
+            position = ep * rows + i * 128 + lax.broadcasted_iota(jnp.int32, (128, 256), 0)
+            share_of = 1.0 / jnp.minimum(position + 1, span).astype(jnp.float32)
+            for q in range(channels // 256):
+                cols = slice(q * 256, (q + 1) * 256)
+                value = normed[tile_rows(i, 0, 128 + reach), cols].astype(jnp.float32)
+                two = value + pltpu.roll(value, 1, 0)
+                four = two + pltpu.roll(two, 2, 0)
+                eight = four + pltpu.roll(four, 4, 0)
+                sixteen = eight + pltpu.roll(eight, 8, 0)
+                window = jnp.where(
+                    tp == 0, two, jnp.where(tp == 1, four, jnp.where(tp == 2, eight, sixteen))
+                )
+                pooled = window[reach:] * share_of - value[reach:]
+                feats[tile_rows(i), cols] = pooled.astype(jnp.bfloat16)
+            projected = jnp.dot(
+                feats[tile_rows(i), :], w_pool[...], preferred_element_type=jnp.float32
+            )
+            mixed_ref[tile_rows(i), :] = (projected * scale_ref[...]).astype(jnp.bfloat16)
+
     own(0)
+    square_sums()
     own(1)
     relay(0)
     own(2)
     relay(1)
     diagonal(0)
+    own(3)
     keep_w.wait()
     for copy in wcopies:
         copy.wait_recv()
@@ -318,29 +427,32 @@
         load.wait()
     complete(0)
     expand(0)
-    own(3)
     relay(2)
     diagonal(1)
     first_hop(0)
+    relay(3)
     complete(1)
     expand(1)
-    relay(3)
     diagonal(2)
     first_hop(1)
     complete(2)
     expand(2)
     diagonal(3)
+    first_hop(2)
     second_hop(0)
-    first_hop(2)
     complete(3)
     expand(3)
+    normalize()
+    first_hop(3)
     second_hop(1)
-    first_hop(3)
     homeward(0)
     homeward(1)
+    halo()
+    pool(0, tiles // 2)
     second_hop(2)
     second_hop(3)
     homeward(2)
+    pool(tiles // 2, tiles)
     homeward(3)
     for k in range(1, GROUPS):
         home[k].wait_recv()
@@ -348,8 +460,18 @@
         copy.wait_send()
 
 
-def paired_experts(
-    moe_in, moe_gain, route_expert, route_weight, gate_weight, up_weight, down_weight
+def paired_step(
+    mixer_in,
+    mixer_gain,
+    pool_weight,
+    pool_scale,
+    moe_in,
+    moe_gain,
+    route_expert,
+    route_weight,
+    gate_weight,
+    up_weight,
+    down_weight,
 ):
     tokens = moe_in.shape[0]
     n_ep, n_tp = lax.axis_size("ep"), lax.axis_size("tp")
@@ -391,11 +513,15 @@
     hbm = pl.BlockSpec(memory_space=pl.ANY)
     dma = pltpu.SemaphoreType.DMA
     model = moe_in.shape[1]
-    fin = pl.pallas_call(
+    rows, channels = mixer_in.shape
+    fin, mixer_out = pl.pallas_call(
         functools.partial(expert_kernel, cap),
-        out_shape=jax.ShapeDtypeStruct((slots, width), jnp.bfloat16),
-        in_specs=[vmem, vmem, hbm, hbm, hbm],
-        out_specs=vmem,
+        out_shape=(
+            jax.ShapeDtypeStruct((slots, width), jnp.bfloat16),
+            jax.ShapeDtypeStruct((rows, channels), jnp.bfloat16),
+        ),
+        in_specs=[vmem, vmem, hbm, hbm, hbm, hbm, vmem, hbm, vmem],
+        out_specs=(vmem, vmem),
         scratch_shapes=[
             pltpu.VMEM((n_tp, n_ep * cap, width), jnp.bfloat16),
             pltpu.VMEM((n_ep, 8, 128), jnp.float32),
@@ -406,27 +532,46 @@
             pltpu.VMEM((GROUPS, 2, 2 * cap, width), jnp.bfloat16),
             pltpu.VMEM((GROUPS, 2, 2 * cap, width), jnp.bfloat16),
             pltpu.VMEM((GROUPS, 2, 2 * cap, width), jnp.bfloat16),
-            pltpu.VMEM((GROUPS, 2 * cap, width), jnp.bfloat16),
-            pltpu.VMEM((GROUPS, cap, width), jnp.bfloat16),
-            dma((5,)),
+            pltpu.VMEM((GROUPS, 2, 2 * cap, width // 2), jnp.bfloat16),
+            pltpu.VMEM((GROUPS, 2, cap, width // 2), jnp.bfloat16),
+            dma((7,)),
             dma((8,)),
             dma((8,)),
             dma((4,)),
             dma((4,)),
-            dma((28,)),
-            dma((28,)),
+            dma((32,)),
+            dma((32,)),
             dma((8,)),
             dma((8,)),
-            dma((16,)),
-            dma((16,)),
+            dma((24,)),
+            dma((24,)),
+            pltpu.VMEM((rows, channels), jnp.bfloat16),
+            pltpu.VMEM(pool_weight.shape[1:], jnp.bfloat16),
+            pltpu.VMEM((rows // 128, 128), jnp.float32),
+            pltpu.VMEM((3, rows // 128, 128), jnp.float32),
+            pltpu.VMEM((rows // 128, 128), jnp.float32),
+            pltpu.VMEM((rows + WINDOW_MAX, channels), jnp.bfloat16),
+            dma((4,)),
+            dma((4,)),
         ],
         compiler_params=pltpu.CompilerParams(
             collective_id=0, has_side_effects=True, vmem_limit_bytes=56 * 1024 * 1024
         ),
-    )(outgoing, wrow, gate_weight[0], up_weight[0], down_weight[0])
-    return lax.dot_general(
+    )(
+        outgoing,
+        wrow,
+        gate_weight[0],
+        up_weight[0],
+        down_weight[0],
+        mixer_in,
+        mixer_gain[None, :],
+        pool_weight[0],
+        pool_scale[None, :],
+    )
+    moe_out = lax.dot_general(
         select, fin, (((0,), (0,)), ((), ())), preferred_element_type=jnp.float32
     ).astype(jnp.bfloat16)
+    return (mixer_out, moe_out)
 
 
 def any_experts(
@@ -476,7 +621,7 @@
     return moe_out
 
 
-def shards(
+def general_step(
     mixer_in,
     mixer_gain,
     pool_weight,
@@ -513,17 +658,16 @@
     mixer_out = (
         jnp.dot(pooled, pool_weight[0], preferred_element_type=jnp.float32) * pool_scale
     ).astype(jnp.bfloat16)
-    paired = lax.axis_size("ep") == 2 * GROUPS and lax.axis_size("tp") == 4
-    experts_of = paired_experts if paired else any_experts
-    moe_out = experts_of(
+    moe_out = any_experts(
         moe_in, moe_gain, route_expert, route_weight, gate_weight, up_weight, down_weight
     )
     return (mixer_out, moe_out)
 
 
 def solution(mesh):
+    paired = mesh.shape["ep"] == 2 * GROUPS and mesh.shape["tp"] == 4
     return jax.shard_map(
-        shards,
+        paired_step if paired else general_step,
         mesh=mesh,
         in_specs=(
             P("ep", "tp"),

time: 129 us -> 96.6 us (0.75)
  other arithmetic: 16.2 us -> 2.86 us
  blocking collectives: 8.38 us -> 0 us
  matrix products: 12.4 us -> 5.9 us
  starting transfers between devices: 3.43 us -> 0 us
  Pallas kernels: 85.6 us -> 83.7 us
    psum x1 -> x0, blocking collectives: 8.38 us -> none  [shards(): squares = lax.psum(jnp.sum(feats * feats, axis=1), 'tp')]
    another operation x1 -> x0, other arithmetic: 7.5 us -> none  [shards(): jnp.stack(totals)]
    dot_general x5 -> x4, matrix products: 12.4 us -> 5.9 us  [the longest x1 2.43 us: paired_step(): jnp.dot(select, normed, preferred_element_type=jnp.float32)]
    convert_element_type x5 -> x2, other arithmetic: 4.35 us -> 0.01 us  [the longest x1 0.01 us: paired_step(): member[:, :, None] * by_expert[:, None, :]]
    ppermute x1 -> x0, starting transfers between devices: 3.43 us -> none  [passed_along(): lax.ppermute(value, axis, [(source, source + steps) for source in range(f...]
    reduce_sum x3 -> x2, other arithmetic: 4.3 us -> 2.09 us  [the longest x1 2.09 us: paired_step(): factor = lax.rsqrt(jnp.mean(feats * feats, axis=1, keepdims=True) + EPS)]
    pallas_call x1, Pallas kernels: 85.6 us -> 83.7 us  [paired_step(): pl.pallas_call(functools.partial(expert_kernel, cap), out_shape=(jax.Shap...]
    unnamed x10 -> x5, local copies, waits for them, and re-layouts: 1.34 us -> 3.09 us
  transfers between devices with their start and end apart: 1 -> 0, of which waited for: 0 -> 0; matrix products, arithmetic and copies ran while one was open for 7% -> 0% of each run, Pallas kernels for 66% -> 0%
where the time goes in v2:
time: 96.6 us; the launch traced here: 96.3 us
  Pallas kernels  83.7 us (87%)
  matrix products  5.9 us (6%)
  local copies, waits for them, and re-layouts  3.09 us (3%)
  other arithmetic  2.86 us (3%)
    pallas_call x1, Pallas kernels, paired_step(): pl.pallas_call(functools.partial(expert_kernel, cap), out_shape=(jax.Shap...  83.7 us
    unnamed x5, local copies, waits for them, and re-layouts  3.09 us
    dot_general x1, matrix products, paired_step(): jnp.dot(select, normed, preferred_element_type=jnp.float32)  2.43 us
    dot_general x1, matrix products, paired_step(): lax.dot_general(select, fin, (((0,), (0,)), ((), ())), preferred_element_...  2.42 us
    reduce_sum x1, other arithmetic, paired_step(): factor = lax.rsqrt(jnp.mean(feats * feats, axis=1, keepdims=True) + EPS)  2.09 us

profile of v2, /device:TPU:0, one launch (start us, length us, event | category | flops | bytes accessed | tf_op | source)
XLA Modules:
  0.0 96.3 jit_solution(18187022903281217739)
XLA Ops:
  0.6 0.0 copy-start
  0.6 0.0 copy-start.1
  0.7 0.0 dynamic-slice-start
  0.7 0.7 and_select_fusion.1
  1.4 0.2 fusion
  1.6 2.1 %multiply_reduce_fusion = f32[256]{0:T(256)S(1)} fusion(bf16[256,4096]{1,0:T(8,128)(2,1)} %param.15), kind=kLoop, calls=%fused_computation | loop fusion | flops 3145472 | bytes 2098176 | tf_op jit(solution)/shard_map/reduce_sum | solution.py:493
  3.7 0.0 dynamic-slice-done
  3.7 2.4 %convolution_convert_fusion.out_ref = bf16[384,1024]{1,0:T(8,128)(2,1)} fusion(f32[1024]{0:T(1024)S(1)} %dynamic-slice-done, f32[256]{0:T(256)S(1)} %add_rsqrt_fusion, bf16[256,4096]{1,0:T(8,128)(2,1)} %param.15, s32[]{:T(128)} %select_n.34, s32[256]{0:T(256)S(1)} %multiply_add_fusion), kind=kOutput, calls=%fused_computation.1 | convolution fusion | flops 202866688 | bytes 1317376 | tf_op jit(solution)/shard_map/dot_general | solution.py:497
  6.2 0.0 copy-done
  6.2 0.0 copy-done.1
  6.2 0.9 fusion.7.wrow_ref
  7.1 83.7 %shard_map.122 = (bf16[384,1024]{1,0:T(8,128)(2,1)}, bf16[1024,1024]{1,0:T(8,128)(2,1)}) custom-call(bf16[384,1024]{1,0:T(8,128)(2,1)} %convolution_convert_fusion.out_ref, f32[4,8,128]{2,1,0:T(8,128)} %fusion.7.wrow_ref, bf16[4096,256]{1,0:T(8,128)(2,1)} %bitcast.19, bf16[4096,256]{1,0:T(8,128)(2,1)} %bitcast.20, bf16[256,4096]{1,0:T(8,128)(2,1)} %bitcast.21, ...), custom_call_target="tpu_custom_call" | custom-call | tf_op jit(solution)/shard_map/pallas_call | solution.py:517
  90.8 2.4 %convolution_convert_fusion.1 = bf16[256,1024]{1,0:T(8,128)(2,1)} fusion(bf16[384,1024]{1,0:T(8,128)(2,1)} %get-tuple-element.5, s32[256]{0:T(256)S(1)} %multiply_add_fusion), kind=kOutput, calls=%fused_computation.2 | convolution fusion | flops 201687040 | bytes 1311744 | tf_op jit(solution)/shard_map/dot_general | solution.py:571
  93.2 3.1 %copy.16 = bf16[1024,1024]{1,0:T(8,128)(2,1)} copy(bf16[1024,1024]{1,0:T(8,128)(2,1)} %get-tuple-element.10) | data formatting | bytes 4194304
  (6 shorter events, 0.0 us)
Async XLA Ops:
  0.6 5.5 %copy-start = (s32[256,2]{0,1:T(2,128)S(1)}, s32[256,2]{0,1:T(2,128)}, u32[]{:S(2)}) copy-start(s32[256,2]{0,1:T(2,128)} %param.17) | copy-start | bytes 6148
  0.6 5.5 %copy-start.1 = (f32[256,2]{0,1:T(2,128)S(1)}, f32[256,2]{0,1:T(2,128)}, u32[]{:S(2)}) copy-start(f32[256,2]{0,1:T(2,128)} %param.18) | copy-start | bytes 6148
  0.7 3.1 %dynamic-slice-start = ((f32[4096]{0:T(1024)}, s32[]{:T(128)}), f32[1024]{0:T(1024)S(1)}, s32[]{:S(2)}) async-start(f32[4096]{0:T(1024)} %param.16, s32[]{:T(128)} %select_n.34), calls=%async_computation | async-start | bytes 8704 | tf_op jit(solution)/shard_map/dynamic_slice | solution.py:495

commit v3 on v2

--- a/solution.py
+++ b/solution.py
@@ -413,10 +413,14 @@
     square_sums()
     own(1)
     relay(0)
+    normalize()
     own(2)
     relay(1)
+    halo()
+    pool(0, tiles // 4)
     diagonal(0)
     own(3)
+    pool(tiles // 4, tiles // 2)
     keep_w.wait()
     for copy in wcopies:
         copy.wait_recv()
@@ -442,18 +446,16 @@
     second_hop(0)
     complete(3)
     expand(3)
-    normalize()
     first_hop(3)
     second_hop(1)
-    homeward(0)
     homeward(1)
-    halo()
-    pool(0, tiles // 2)
     second_hop(2)
     second_hop(3)
     homeward(2)
-    pool(tiles // 2, tiles)
+    pool(tiles // 2, 5 * tiles // 8)
     homeward(3)
+    homeward(0)
+    pool(5 * tiles // 8, tiles)
     for k in range(1, GROUPS):
         home[k].wait_recv()
     for copy in started:

time: 96.6 us -> 95.6 us (0.990)
  Pallas kernels: 83.7 us -> 82.7 us
    pallas_call x1, Pallas kernels: 83.7 us -> 82.7 us  [paired_step(): pl.pallas_call(functools.partial(expert_kernel, cap), out_shape=(jax.Shap...]
where the time goes in v3:
time: 95.6 us; the launch traced here: 95.2 us
  Pallas kernels  82.7 us (87%)
  matrix products  5.9 us (6%)
  local copies, waits for them, and re-layouts  3.09 us (3%)
  other arithmetic  2.86 us (3%)
    pallas_call x1, Pallas kernels, paired_step(): pl.pallas_call(functools.partial(expert_kernel, cap), out_shape=(jax.Shap...  82.7 us
    unnamed x5, local copies, waits for them, and re-layouts  3.09 us
    dot_general x1, matrix products, paired_step(): jnp.dot(select, normed, preferred_element_type=jnp.float32)  2.43 us
    dot_general x1, matrix products, paired_step(): lax.dot_general(select, fin, (((0,), (0,)), ((), ())), preferred_element_...  2.42 us
    reduce_sum x1, other arithmetic, paired_step(): factor = lax.rsqrt(jnp.mean(feats * feats, axis=1, keepdims=True) + EPS)  2.09 us

profile of v3, /device:TPU:0, one launch (start us, length us, event | category | flops | bytes accessed | tf_op | source)
XLA Modules:
  0.0 95.2 jit_solution(16192861686082265667)
XLA Ops:
  0.6 0.0 copy-start
  0.6 0.0 copy-start.1
  0.7 0.0 dynamic-slice-start
  0.7 0.7 and_select_fusion.1
  1.4 0.2 fusion
  1.6 2.1 %multiply_reduce_fusion = f32[256]{0:T(256)S(1)} fusion(bf16[256,4096]{1,0:T(8,128)(2,1)} %param.15), kind=kLoop, calls=%fused_computation | loop fusion | flops 3145472 | bytes 2098176 | tf_op jit(solution)/shard_map/reduce_sum | solution.py:495
  3.7 0.0 dynamic-slice-done
  3.7 2.4 %convolution_convert_fusion.out_ref = bf16[384,1024]{1,0:T(8,128)(2,1)} fusion(f32[1024]{0:T(1024)S(1)} %dynamic-slice-done, f32[256]{0:T(256)S(1)} %add_rsqrt_fusion, bf16[256,4096]{1,0:T(8,128)(2,1)} %param.15, s32[]{:T(128)} %select_n.34, s32[256]{0:T(256)S(1)} %multiply_add_fusion), kind=kOutput, calls=%fused_computation.1 | convolution fusion | flops 202866688 | bytes 1317376 | tf_op jit(solution)/shard_map/dot_general | solution.py:499
  6.2 0.0 copy-done
  6.2 0.0 copy-done.1
  6.2 0.9 fusion.7.wrow_ref
  7.1 82.7 %shard_map.122 = (bf16[384,1024]{1,0:T(8,128)(2,1)}, bf16[1024,1024]{1,0:T(8,128)(2,1)}) custom-call(bf16[384,1024]{1,0:T(8,128)(2,1)} %convolution_convert_fusion.out_ref, f32[4,8,128]{2,1,0:T(8,128)} %fusion.7.wrow_ref, bf16[4096,256]{1,0:T(8,128)(2,1)} %bitcast.19, bf16[4096,256]{1,0:T(8,128)(2,1)} %bitcast.20, bf16[256,4096]{1,0:T(8,128)(2,1)} %bitcast.21, ...), custom_call_target="tpu_custom_call" | custom-call | tf_op jit(solution)/shard_map/pallas_call | solution.py:519
  89.7 2.4 %convolution_convert_fusion.1 = bf16[256,1024]{1,0:T(8,128)(2,1)} fusion(bf16[384,1024]{1,0:T(8,128)(2,1)} %get-tuple-element.5, s32[256]{0:T(256)S(1)} %multiply_add_fusion), kind=kOutput, calls=%fused_computation.2 | convolution fusion | flops 201687040 | bytes 1311744 | tf_op jit(solution)/shard_map/dot_general | solution.py:573
  92.2 3.1 %copy.16 = bf16[1024,1024]{1,0:T(8,128)(2,1)} copy(bf16[1024,1024]{1,0:T(8,128)(2,1)} %get-tuple-element.10) | data formatting | bytes 4194304
  (6 shorter events, 0.0 us)
Async XLA Ops:
  0.6 5.5 %copy-start = (s32[256,2]{0,1:T(2,128)S(1)}, s32[256,2]{0,1:T(2,128)}, u32[]{:S(2)}) copy-start(s32[256,2]{0,1:T(2,128)} %param.17) | copy-start | bytes 6148
  0.6 5.5 %copy-start.1 = (f32[256,2]{0,1:T(2,128)S(1)}, f32[256,2]{0,1:T(2,128)}, u32[]{:S(2)}) copy-start(f32[256,2]{0,1:T(2,128)} %param.18) | copy-start | bytes 6148
  0.7 3.1 %dynamic-slice-start = ((f32[4096]{0:T(1024)}, s32[]{:T(128)}), f32[1024]{0:T(1024)S(1)}, s32[]{:S(2)}) async-start(f32[4096]{0:T(1024)} %param.16, s32[]{:T(128)} %select_n.34), calls=%async_computation | async-start | bytes 8704 | tf_op jit(solution)/shard_map/dynamic_slice | solution.py:497
